TPU v7x, 32 devices: a whole 2x2x4 slice. The times are simulated.
32 devices in a mesh: grp: 2 (over y), ep: 4 (over z), tp: 4 (over x, core).
Axes of the slice: x: 2, y: 2, z: 4, core: 2. Of those that a mesh axis runs over, the one named last changes fastest.
Arguments:
- memory_query_rows: bfloat16 [1024, 1024], P(('grp', 'ep'), 'tp'), parts along dimension 0, may hold values from -6 to 6
- memory_key_rows: bfloat16 [1024, 1024], P(('grp', 'ep'), 'tp'), parts along dimension 0, may hold values from -6 to 6
- memory_value_rows: bfloat16 [1024, 1024], P(('grp', 'ep'), 'tp'), parts along dimension 0, may hold values from -6 to 6
- input_gate_log: float32 [8, 1024], P('tp', ('grp', 'ep')), parts along dimension 1, may hold values from -4 to 300
- forget_gate_logits: float32 [8, 1024], P('tp', ('grp', 'ep')), parts along dimension 1
- forget_log_extra: float32 [8, 1024], P('tp', ('grp', 'ep')), parts along dimension 1, may hold values from -1.5 to 0
- memory_output_weight: bfloat16 [1024, 2048], P(None, 'tp'), may hold values from -0.1875 to 0.1875
- second_batch_tokens: bfloat16 [4096, 2048], P(('grp', 'ep', 'tp')), parts along dimension 0, may hold values from -6 to 6
- expert_norm_gain: float32 [2048], replicated, may hold values from 0.1 to 1.9
- routing_expert_index: int32 [4096, 2], P(('grp', 'ep', 'tp')), parts along dimension 0, may hold values from 0 to 3, all different within a row; in each aligned block of 128 rows (0 to 127, 128 to 255, ...) at most 80 rows name the same one
- routing_expert_weight: float32 [4096, 2], P(('grp', 'ep', 'tp')), parts along dimension 0, may hold values from 0.2 to 1
- expert_gate_matrix: bfloat16 [4, 2048, 3584], P('ep', None, 'tp'), may hold values from -0.125 to 0.125
- expert_up_matrix: bfloat16 [4, 2048, 3584], P('ep', None, 'tp'), may hold values from -0.125 to 0.125
- expert_down_matrix: bfloat16 [4, 3584, 2048], P('ep', 'tp'), may hold values from -0.09375 to 0.09375
Outputs:
- mixed_out: bfloat16 [1024, 2048], P(('grp', 'ep'), 'tp'), parts along dimension 0
- expert_out: bfloat16 [4096, 2048], P(('grp', 'ep', 'tp')), parts along dimension 0
There are 2 independent parts, one for each index of `grp`. A program takes and returns all parts, laid end to end along the dimension named above; an argument that names none is the same for every part. Nothing has to cross between parts.
Inputs may be any that keep to these rules, and one draw needn't show every extreme that they name: `routing_expert_index`: within the rows of one device no expert is named by more than 80 rows, a bound that some block reaches; the 2 experts of a row differ.
All inputs are finite; a program needn't handle non-finite values.
Results may differ from a plain program's by a relative error of at most 0.012.
The roundings to bfloat16 on the way count: a program that leaves them out, or rounds other values in their place, can miss the bound.
Values may be sent and summed in bfloat16 or wider, within the bound.
A program may use at most 128 MiB of HBM per device.

v0:
```python
import jax
import jax.numpy as jnp
from jax import lax
from jax.sharding import PartitionSpec as P

DH = 128
TOP = 2
BLOCK = 128


neg_big = -1e30
rms_eps = 1e-06
highest = lax.Precision.HIGHEST


def entering(part, axis, combine, identity):
    place = lax.axis_index(axis)
    gathered = jax.tree.map(lambda a: lax.all_gather(a, axis), part)
    state = jax.tree.map(lambda a, e: jnp.zeros_like(a) + jnp.asarray(e, a.dtype), part, identity)

    def one(turn, state):
        return combine(
            state, jax.tree.map(lambda a: lax.dynamic_index_in_dim(a, turn, 0, False), gathered)
        )

    return lax.fori_loop(0, place, one, state)


def state_update(state_in, inputs, cumulative):
    memory, normer, stabilizer = state_in
    key_rows, values, in_gate, forget = inputs
    block_total = cumulative[:, -1]
    weights = block_total[:, None] - cumulative + in_gate
    new_stab = jnp.maximum(block_total + stabilizer, jnp.max(weights, axis=-1))
    scaled = jnp.exp(weights - new_stab[:, None])
    retained = jnp.exp(block_total + stabilizer - new_stab)
    weighted_keys = scaled[:, :, None] * key_rows
    memory = retained[:, None, None] * memory + jnp.einsum(
        "hsd,hse->hde", weighted_keys, values, precision=highest
    )
    normer = retained[:, None] * normer + jnp.sum(weighted_keys, axis=1)
    return (memory, normer, new_stab)


def state_only(state_in, inputs):
    cumulative = jnp.cumsum(inputs[3], axis=-1)
    return (state_update(state_in, inputs, cumulative), None)


def block_step(state_in, inputs):
    memory, normer, stabilizer = state_in
    queries, key_rows, values, in_gate, forget = inputs
    length = queries.shape[1]
    causal = jnp.tril(jnp.ones((length, length), dtype=bool))
    cumulative = jnp.cumsum(forget, axis=-1)
    decays = jnp.where(
        causal, cumulative[:, :, None] - cumulative[:, None, :] + in_gate[:, None, :], -jnp.inf
    )
    carried_max = cumulative + stabilizer[:, None]
    row_max = jnp.maximum(jnp.max(decays, axis=-1), carried_max)
    scores = jnp.einsum("htd,hsd->hts", queries, key_rows, precision=highest) * jnp.exp(
        decays - row_max[:, :, None]
    )
    carried = jnp.exp(carried_max - row_max)
    numerator = carried[:, :, None] * jnp.einsum(
        "htd,hde->hte", queries, memory, precision=highest
    ) + jnp.einsum("hts,hse->hte", scores, values, precision=highest)
    denominator = carried * jnp.einsum("htd,hd->ht", queries, normer, precision=highest) + jnp.sum(
        scores, axis=-1
    )
    output = numerator / jnp.maximum(jnp.abs(denominator), jnp.exp(-row_max))[:, :, None]
    new_state = state_update(state_in, (key_rows, values, in_gate, forget), cumulative)
    return (new_state, output)


def join_states(earlier, later):
    mem_early, norm_early, stab_early, total_early = earlier
    mem_late, norm_late, stab_late, total_late = later
    stabilizer = jnp.maximum(total_late + stab_early, stab_late)
    early_scale = jnp.exp(total_late + stab_early - stabilizer)
    late_scale = jnp.exp(stab_late - stabilizer)
    memory = early_scale[:, None, None] * mem_early + late_scale[:, None, None] * mem_late
    normer = early_scale[:, None] * norm_early + late_scale[:, None] * norm_late
    return (memory, normer, stabilizer, total_early + total_late)


def split_blocks(row_block, heads):
    count = row_block.shape[0] // BLOCK
    return row_block.astype(jnp.float32).reshape(count, BLOCK, heads, -1).transpose(0, 2, 1, 3)


def gate_blocks(gate_rows):
    heads = gate_rows.shape[0]
    return gate_rows.reshape(heads, -1, BLOCK).transpose(1, 0, 2)


def route_slots(routing_expert_index, experts, capacity):
    flat_ids = routing_expert_index.reshape(-1)
    onehot = (flat_ids[:, None] == jnp.arange(experts, dtype=jnp.int32)[None, :]).astype(jnp.int32)
    route_ranks = jnp.sum((jnp.cumsum(onehot, axis=0) - 1) * onehot, axis=1)
    return (flat_ids * capacity + route_ranks).reshape(routing_expert_index.shape)


def on_device(
    memory_query_rows,
    memory_key_rows,
    memory_value_rows,
    input_gate_log,
    forget_gate_logits,
    forget_log_extra,
    memory_output_weight,
    second_batch_tokens,
    expert_norm_gain,
    routing_expert_index,
    routing_expert_weight,
    expert_gate_matrix,
    expert_up_matrix,
    expert_down_matrix,
):
    heads_local = input_gate_log.shape[0]
    positions = input_gate_log.shape[1]
    queries = split_blocks(memory_query_rows, heads_local)
    key_rows = split_blocks(memory_key_rows, heads_local) * DH ** (-0.5)
    values = split_blocks(memory_value_rows, heads_local)
    in_gate = gate_blocks(input_gate_log)
    forget_log_value = jax.nn.log_sigmoid(forget_gate_logits) + forget_log_extra
    forget = gate_blocks(forget_log_value)
    zero_memory = jnp.zeros((heads_local, DH, DH), jnp.float32)
    zero_normer = jnp.zeros((heads_local, DH), jnp.float32)
    low_stab = jnp.full((heads_local,), neg_big, jnp.float32)
    local_state, _ = lax.scan(
        state_only, (zero_memory, zero_normer, low_stab), (key_rows, values, in_gate, forget)
    )
    totals = jnp.sum(forget_log_value, axis=1)
    identity = (zero_memory, zero_normer, low_stab, jnp.zeros((heads_local,), jnp.float32))
    mem_prior, norm_prior, stab_prior, total_prior = entering(
        (local_state[0], local_state[1], local_state[2], totals), "ep", join_states, identity
    )
    stab_in = jnp.maximum(total_prior, stab_prior)
    factor = jnp.exp(stab_prior - stab_in)
    incoming = (factor[:, None, None] * mem_prior, factor[:, None] * norm_prior, stab_in)
    _, outputs = lax.scan(block_step, incoming, (queries, key_rows, values, in_gate, forget))
    memory_rows = outputs.transpose(0, 2, 1, 3).reshape(positions, -1).astype(jnp.bfloat16)
    mixed = jnp.dot(
        lax.all_gather(memory_rows, "tp", axis=1, tiled=True),
        memory_output_weight,
        preferred_element_type=jnp.float32,
    )
    mixed_out = mixed.astype(jnp.bfloat16)
    tok_rows = second_batch_tokens.shape[0]
    experts = lax.axis_size("ep")
    capacity = max(2, 5 * tok_rows * TOP // (4 * experts))
    slots_dev = experts * capacity
    tokens_f = second_batch_tokens.astype(jnp.float32)
    normed = (
        tokens_f
        * lax.rsqrt(jnp.mean(tokens_f * tokens_f, axis=1, keepdims=True) + rms_eps)
        * expert_norm_gain
    ).astype(jnp.bfloat16)
    slot_ids = route_slots(routing_expert_index, experts, capacity)
    slot_table = jnp.arange(slots_dev, dtype=jnp.int32)
    placing = jnp.zeros((slots_dev, tok_rows), jnp.bfloat16)
    for column in range(TOP):
        placing = placing + (slot_table[:, None] == slot_ids[None, :, column]).astype(jnp.bfloat16)
    outgoing = jnp.dot(placing, normed, preferred_element_type=jnp.float32).astype(jnp.bfloat16)
    gate_weight = expert_gate_matrix[0]
    up_weight = expert_up_matrix[0]
    down_weight = expert_down_matrix[0]
    arrived = lax.all_to_all(outgoing, "ep", split_axis=0, concat_axis=0, tiled=True)
    row_block = lax.all_gather(arrived, "tp", axis=0, tiled=True)
    gate_act = jnp.dot(row_block, gate_weight, preferred_element_type=jnp.float32)
    up_act = jnp.dot(row_block, up_weight, preferred_element_type=jnp.float32)
    hidden = (jax.nn.silu(gate_act) * up_act).astype(jnp.bfloat16)
    terms = (
        jnp.dot(hidden, down_weight, preferred_element_type=jnp.float32)
        .astype(jnp.bfloat16)
        .astype(jnp.float32)
    )
    summed = lax.psum_scatter(terms.astype(jnp.bfloat16), "tp", scatter_dimension=0, tiled=True)
    returned = lax.all_to_all(summed, "ep", split_axis=0, concat_axis=0, tiled=True)
    picked = returned[slot_ids.reshape(-1)].astype(jnp.float32).reshape(tok_rows, TOP, -1)
    expert_out = jnp.sum(picked * routing_expert_weight[:, :, None], axis=1).astype(jnp.bfloat16)
    return (mixed_out, expert_out)


def solution(mesh):
    placed = (
        P(("grp", "ep"), "tp"),
        P(("grp", "ep"), "tp"),
        P(("grp", "ep"), "tp"),
        P("tp", ("grp", "ep")),
        P("tp", ("grp", "ep")),
        P("tp", ("grp", "ep")),
        P(None, "tp"),
        P(("grp", "ep", "tp"), None),
        P(),
        P(("grp", "ep", "tp"), None),
        P(("grp", "ep", "tp"), None),
        P("ep", None, "tp"),
        P("ep", None, "tp"),
        P("ep", "tp", None),
    )
    return jax.shard_map(
        on_device,
        mesh=mesh,
        in_specs=placed,
        out_specs=(P(("grp", "ep"), "tp"), P(("grp", "ep", "tp"), None)),
        check_vma=False,
    )
```

profile of v0, /device:TPU:0, one launch (start us, length us, event | category | flops | bytes accessed | tf_op | source)
XLA Modules:
  0.0 221.1 jit_solution(15957538054483665191)
XLA Ops:
  7.2 0.9 copy.71
  8.1 0.1 eq.60
  8.2 0.1 eq.56
  8.4 1.2 reduce-window.6
  9.7 0.1 copy.74
  9.8 0.1 copy.75
  9.9 0.1 add_bitcast_fusion
  10.0 0.1 reduce_sum.72
  10.2 0.2 slice_reduce_fusion.1
  10.4 1.2 fusion.15
  11.6 1.6 convolution_convert_fusion.1
  13.3 37.6 %all_to_all.24 = bf16[4,80,2048]{2,1,0:T(8,128)(2,1)} all-to-all(bf16[4,80,2048]{2,1,0:T(8,128)(2,1)S(1)} %bitcast.140), channel_id=1, replica_groups=mesh['grp'=2,'ep'=4,'tp'=4] {'ep'}, dimensions={0} | all-to-all | bytes 2621440 | tf_op jit(solution)/shard_map/all_to_all | solution.py:169
  50.9 39.7 %all-gather.5.cloned.1.call-done = bf16[1280,2048]{1,0:T(8,128)(2,1)} async-done(((bf16[320,2048]{1,0:T(8,128)(2,1)}), bf16[1280,2048]{1,0:T(8,128)(2,1)}) %all-gather.5.cloned.1.call-update) | async-done | bytes 5242896 | tf_op jit(solution)/shard_map/all_gather | solution.py:170
  90.6 10.0 %fusion.9 = f32[1280,896]{1,0:T(8,128)} fusion(bf16[1280,2048]{1,0:T(8,128)(2,1)} %all-gather.5.cloned.1.call-done, bf16[1,2048,896]{2,1,0:T(8,128)(2,1)} %param.27), kind=kOutput, calls=%fused_computation.18 | convolution fusion | flops 4697620480 | bytes 13500416 | tf_op jit(solution)/shard_map/dot_general | solution.py:171
  100.6 17.5 %convolution_convert_fusion = bf16[1280,2048]{1,0:T(8,128)(2,1)} fusion(bf16[1,896,2048]{2,1,0:T(8,128)(2,1)} %param.29, f32[1280,896]{1,0:T(8,128)} %fusion.9, bf16[1280,2048]{1,0:T(8,128)(2,1)} %all-gather.5.cloned.1.call-done, bf16[1,2048,896]{2,1,0:T(8,128)(2,1)} %param.28), kind=kOutput, calls=%fused_computation.14 | convolution fusion | flops 9404743680 | bytes 22413312 | tf_op jit(solution)/shard_map/dot_general | solution.py:175
  118.2 0.6 copy-done.6
  118.8 0.1 fusion.54
  118.9 0.3 reduce_window_sum.27
  119.2 0.2 slice_reduce_fusion.2
  119.4 0.2 fusion.53
  119.6 0.1 copy.62
  119.7 0.6 dynamic-slice.4
  120.9 0.2 multiply_reduce_fusion.1
  121.2 0.2 dynamic-update-slice
  121.4 10.9 %all-gather.2 = f32[4,1,2]{2,1,0:T(1,128)S(1)} all-gather(f32[1,1,2]{2,1,0:T(1,128)S(1)} %fusion.48), channel_id=1, replica_groups=mesh['grp'=2,'ep'=4,'tp'=4] {'ep'}, dimensions={0}, use_global_device_ids=true | all-gather | bytes 40 | tf_op jit(solution)/shard_map/all_gather | solution.py:18
  132.3 8.4 %all-reduce = f32[8]{0:T(128)S(1)} all-reduce(f32[8]{0:T(128)S(1)} %dynamic-update-slice), channel_id=2, replica_groups=mesh['grp'=2,'ep'=4,'tp'=4] {'ep'}, use_global_device_ids=true, to_apply=%add | all-reduce | flops 8 | bytes 64
  140.8 0.1 copy.84
  140.9 0.1 reshape.209
  141.0 0.1 mul.232
  141.1 0.1 copy.76
  141.3 0.1 fusion.26
  141.5 9.6 %all_gather.31 = f32[4,2,128]{2,1,0:T(2,128)S(1)} all-gather(f32[1,2,128]{2,1,0:T(2,128)S(1)} %bitcast_add_fusion), channel_id=1, replica_groups=mesh['grp'=2,'ep'=4,'tp'=4] {'ep'}, dimensions={0}, use_global_device_ids=true | all-gather | bytes 5120 | tf_op jit(solution)/shard_map/all_gather | solution.py:18
  151.1 0.1 fusion.25
  151.3 0.4 convolution_add_fusion.1
  151.6 15.3 %all-gather.1 = f32[8,128,128]{2,1,0:T(8,128)S(1)} all-gather(f32[2,128,128]{2,1,0:T(8,128)S(1)} %convolution_add_fusion.1), channel_id=3, replica_groups=mesh['grp'=2,'ep'=4,'tp'=4] {'ep'}, dimensions={0}, use_global_device_ids=true | all-gather | bytes 655360 | tf_op jit(solution)/shard_map/all_gather | solution.py:18
  167.0 2.6 %reduce-scatter.2.cloned.1.call-done = bf16[320,2048]{1,0:T(8,128)(2,1)} async-done(((bf16[1280,2048]{1,0:T(8,128)(2,1)}), bf16[320,2048]{1,0:T(8,128)(2,1)}) %reduce-scatter.2.cloned.1.call-update) | async-done | bytes 1310736 | tf_op jit(solution)/shard_map/reduce_scatter | solution.py:179
  169.7 4.6 %all-to-all-start.1 = ((bf16[4,80,2048]{2,1,0:T(8,128)(2,1)}), bf16[4,80,2048]{2,1,0:T(8,128)(2,1)S(1)}, u32[]{:S(2)}, u32[]{:S(2)}) async-start(bf16[4,80,2048]{2,1,0:T(8,128)(2,1)} %bitcast.142), calls=%async_computation.2 | async-start | bytes 2621440 | tf_op jit(solution)/shard_map/all_to_all | solution.py:180
  174.4 0.2 fusion.34
  174.5 0.3 fusion.56
  174.9 0.1 exponential_maximum_fusion
  174.9 0.4 fusion.12
  175.3 0.2 fusion.14
  175.5 6.0 %all_gather.32 = bf16[128,1024]{0,1:T(8,128)(2,1)S(1)} all-gather(bf16[128,256]{0,1:T(8,128)(2,1)S(1)} %bitcast.145), channel_id=1, replica_groups=mesh['grp'=2,'ep'=4,'tp'=4] {'tp'}, dimensions={1}, use_global_device_ids=true | all-gather | bytes 327680 | tf_op jit(solution)/shard_map/all_gather | solution.py:145
  181.5 1.0 convolution_convert_fusion.2
  182.5 23.0 %all-to-all-done.1 = bf16[4,80,2048]{2,1,0:T(8,128)(2,1)S(1)} async-done(((bf16[4,80,2048]{2,1,0:T(8,128)(2,1)}), bf16[4,80,2048]{2,1,0:T(8,128)(2,1)S(1)}, u32[]{:S(2)}, u32[]{:S(2)}) %all-to-all-start.1) | async-done | bytes 1310752 | tf_op jit(solution)/shard_map/all_to_all | solution.py:180
  205.5 2.3 %gather_fusion = bf16[256,2048]{1,0:T(8,128)(2,1)} fusion(bf16[320,2048]{1,0:T(8,128)(2,1)S(1)} %bitcast.138, s32[1024]{0:T(1024)S(1)} %pad_clamp_fusion), kind=kCustom, calls=%fused_computation | custom fusion | bytes 2098176 | tf_op jit(solution)/shard_map/gather | solution.py:181
  207.8 2.4 %reshape.200 = f32[128,2,2048]{2,1,0:T(2,128)S(1)} reshape(bf16[256,2048]{1,0:T(8,128)(2,1)} %gather_fusion) | data formatting | bytes 3145728 | tf_op jit(solution)/shard_map/convert_element_type | solution.py:181
  210.2 4.0 %multiply_reduce_fusion = bf16[128,2048]{1,0:T(8,128)(2,1)} fusion(f32[128,2,2048]{2,1,0:T(2,128)S(1)} %reshape.200, f32[128,2]{1,0:T(8,128)S(1)} %copy.76), kind=kLoop, calls=%fused_computation.21 | loop fusion | flops 786432 | bytes 2622464 | tf_op jit(solution)/shard_map/reduce_sum | solution.py:182
  (46 shorter events, 0.7 us)
Async XLA Ops:
  7.2 174.3 %copy-start = (bf16[1024,512]{1,0:T(8,128)(2,1)S(1)}, bf16[1024,512]{1,0:T(8,128)(2,1)}, u32[]{:S(2)}) copy-start(bf16[1024,512]{1,0:T(8,128)(2,1)} %param.22) | copy-start | bytes 3145732
  7.2 83.4 %all-gather.5.cloned.1.call-start = ((), (), s32[]{:S(2)}) async-start(), calls=%async_computation.3 | async-start | bytes 6553600 | tf_op jit(solution)/shard_map/all_gather | solution.py:170
  50.9 118.8 %reduce-scatter.2.cloned.1.call-start = ((), (), s32[]{:S(2)}) async-start(), calls=%async_computation.4 | async-start | bytes 6553600 | tf_op jit(solution)/shard_map/reduce_scatter | solution.py:179
  118.1 0.7 copy-start.6
  118.1 0.7 copy-start.7
  118.1 1.3 copy-start.4
  118.1 1.6 copy-start.8
  118.1 22.5 %copy-start.1 = (bf16[128,256]{1,0:T(8,128)(2,1)S(1)}, bf16[128,256]{1,0:T(8,128)(2,1)}, u32[]{:S(2)}) copy-start(bf16[128,256]{1,0:T(8,128)(2,1)} %param.17) | copy-start | bytes 196612
  118.1 22.6 %copy-start.2 = (bf16[128,256]{1,0:T(8,128)(2,1)S(1)}, bf16[128,256]{1,0:T(8,128)(2,1)}, u32[]{:S(2)}) copy-start(bf16[128,256]{1,0:T(8,128)(2,1)} %param.18) | copy-start | bytes 196612
  118.1 22.8 %copy-start.3 = (bf16[128,256]{1,0:T(8,128)(2,1)S(1)}, bf16[128,256]{1,0:T(8,128)(2,1)}, u32[]{:S(2)}) copy-start(bf16[128,256]{1,0:T(8,128)(2,1)} %param.16) | copy-start | bytes 196612
  118.2 23.0 %copy-start.5 = (f32[128,2]{0,1:T(2,128)S(1)}, f32[128,2]{0,1:T(2,128)}, u32[]{:S(2)}) copy-start(f32[128,2]{0,1:T(2,128)} %param.26) | copy-start | bytes 3076
  169.7 35.8 %all-to-all-start.1 = ((bf16[4,80,2048]{2,1,0:T(8,128)(2,1)}), bf16[4,80,2048]{2,1,0:T(8,128)(2,1)S(1)}, u32[]{:S(2)}, u32[]{:S(2)}) async-start(bf16[4,80,2048]{2,1,0:T(8,128)(2,1)} %bitcast.142), calls=%async_computation.2 | async-start | bytes 2621440 | tf_op jit(solution)/shard_map/all_to_all | solution.py:180
Sparse Core Ops, SparseCore 0:
  51.0 39.5 all-gather.4
  118.3 51.3 reduce-scatter.1
where the time goes:
time: 222 us; the launch traced here: 221 us
  blocking collectives  87.7 us (40%)
  waiting for transfers between devices  65.3 us (29%)
  matrix products  31.6 us (14%)
  between operations  15 us (7%)
  local copies, waits for them, and re-layouts  8.75 us (4%)
  other arithmetic  8.13 us (4%)
  starting transfers between devices  4.68 us (2%)
    all_gather x1, waiting for transfers between devices, on_device(): row_block = lax.all_gather(arrived, 'tp', axis=0, tiled=True)  39.7 us
    all_to_all x1, blocking collectives, on_device(): lax.all_to_all(outgoing, 'ep', split_axis=0, concat_axis=0, tiled=True)  37.6 us
    all_gather x3, blocking collectives, entering(): gathered = jax.tree.map(lambda a: lax.all_gather(a, axis), part)  35.8 us
    all_to_all x1, waiting for transfers between devices, on_device(): lax.all_to_all(summed, 'ep', split_axis=0, concat_axis=0, tiled=True)  23 us
    dot_general x1, matrix products, on_device(): jnp.dot(hidden, down_weight, preferred_element_type=jnp.float32)  17.5 us
    dot_general x1, matrix products, on_device(): jnp.dot(row_block, gate_weight, preferred_element_type=jnp.float32)  9.98 us
    unnamed x1, blocking collectives  8.36 us
    all_gather x1, blocking collectives, on_device(): lax.all_gather(memory_rows, 'tp', axis=1, tiled=True)  5.96 us
  transfers between devices with their start and end apart: 3, of which 3 were waited for; matrix products, arithmetic and copies ran while one was open for 3% of the time, Pallas kernels for 0%

commit v1 on v0

v1 whole, which is shorter than its diff:
```python
import functools

import jax
import jax.numpy as jnp
from jax import lax
from jax.experimental import pallas as pl
from jax.experimental.pallas import tpu as pltpu
from jax.sharding import PartitionSpec as P

DH = 128
TOP = 2
BLOCK = 128


neg_big = -1e30
rms_eps = 1e-06
highest = lax.Precision.HIGHEST


MESH = pl.DeviceIdType.MESH
LANES = 128


def expert_kernel(
    ep,
    tp,
    cap,
    out_ref,
    state_ref,
    gate_hbm,
    up_hbm,
    down_hbm,
    ret_ref,
    states_ref,
    gate_up,
    down,
    rows,
    hidden,
    part,
    near_part,
    pair_sum,
    far_part,
    result,
    w_sem,
    own_sem,
    st_sem,
    z_sem,
    far_sem,
    near_sem,
    relay_sem,
    np_sem,
    fp_sem,
    r_sem,
):
    e = lax.axis_index("ep")
    t = lax.axis_index("tp")
    side, core = t // 2, t % 2
    near = side * 2 + (1 - core)
    far = (1 - side) * 2 + core
    tiles = gate_up.shape[0]
    width = rows.shape[2]

    def place(side_at, core_at):
        return pl.ds(pl.multiple_of((core_at * 2 + side_at) * cap, cap), cap)

    mine = place(side, core)
    theirs = place(1 - side, core)

    def remote(src, dst, sems, k, target):
        return pltpu.make_async_remote_copy(
            src_ref=src,
            dst_ref=dst,
            send_sem=sems.at[0, k],
            recv_sem=sems.at[1, k],
            device_id=target,
            device_id_type=MESH,
        )

    def ahead(k):
        return {"ep": lax.rem(e + k, ep)}

    def behind(k):
        return {"ep": lax.rem(e + ep - k, ep)}

    def weight_copies(i):
        cols = pl.ds(pl.multiple_of(i * LANES, LANES), LANES)
        return (
            pltpu.make_async_copy(
                gate_hbm.at[0, :, cols], gate_up.at[i, :, pl.ds(0, LANES)], w_sem.at[0, i]
            ),
            pltpu.make_async_copy(
                up_hbm.at[0, :, cols], gate_up.at[i, :, pl.ds(LANES, LANES)], w_sem.at[1, i]
            ),
        )

    down_copy = pltpu.make_async_copy(down_hbm.at[0], down, own_sem.at[1])
    own_copy = pltpu.make_async_copy(out_ref.at[0], rows.at[0, mine], own_sem.at[0])

    def z_copy(k):
        return remote(out_ref.at[k], rows.at[k, mine], z_sem, k, ahead(k))

    def state_copy(k):
        return remote(state_ref, states_ref.at[k], st_sem, k, ahead(k))

    def far_copy(k):
        return remote(rows.at[k, mine], rows.at[k, mine], far_sem, k, {"tp": far})

    def near_copy(k):
        return remote(rows.at[k, mine], rows.at[k, mine], near_sem, k, {"tp": near})

    def relay_copy(k):
        return remote(rows.at[k, theirs], rows.at[k, theirs], relay_sem, k, {"tp": near})

    def near_part_copy(k):
        span = pl.ds(pl.multiple_of((1 - core) * 2 * cap, 2 * cap), 2 * cap)
        return remote(part.at[k, span], near_part.at[k], np_sem, k, {"tp": near})

    def far_part_copy(k):
        return remote(pair_sum.at[k], far_part.at[k], fp_sem, k, {"tp": far})

    def return_copy(k):
        return remote(result.at[k], ret_ref.at[k], r_sem, k, behind(k))

    barrier = pltpu.get_barrier_semaphore()

    @pl.loop(1, ep)
    def _(k):
        pl.semaphore_signal(barrier, inc=1, device_id=ahead(k), device_id_type=MESH)

    for target in (near, far):
        pl.semaphore_signal(barrier, inc=1, device_id={"tp": target}, device_id_type=MESH)
    own_copy.start()
    pl.semaphore_wait(barrier, ep + 1)

    @pl.loop(1, ep)
    def _(k):
        @pl.when(e + k < ep)
        def _():
            state_copy(k).start()

    @pl.loop(1, ep)
    def _(k):
        z_copy(k).start()

    own_copy.wait()
    far_copy(0).start()
    near_copy(0).start()

    @pl.loop(0, tiles)
    def _(i):
        for copy in weight_copies(i):
            copy.start()

    down_copy.start()

    def feed_forward(k):
        @pl.loop(0, tiles)
        def _(i):
            both = jnp.dot(rows[k], gate_up[i], preferred_element_type=jnp.float32)
            act, up_act = both[:, :LANES], both[:, LANES:]
            hidden[:, pl.ds(pl.multiple_of(i * LANES, LANES), LANES)] = (
                jax.nn.silu(act) * up_act
            ).astype(jnp.bfloat16)

        @pl.when(k == 0)
        def _():
            down_copy.wait()

        @pl.loop(0, width // 256)
        def _(i):
            cols = pl.ds(pl.multiple_of(i * 256, 256), 256)
            part[k, :, cols] = jnp.dot(
                hidden[...], down[:, cols], preferred_element_type=jnp.float32
            ).astype(jnp.bfloat16)

    def pair_stage(k):
        near_part_copy(k).wait_recv()
        other = pl.ds(pl.multiple_of((1 - side) * cap, cap), cap)
        pair_sum[k] = (
            part[k, theirs].astype(jnp.float32) + near_part[k, other].astype(jnp.float32)
        ).astype(jnp.bfloat16)
        far_part_copy(k).start()

    def final_stage(k):
        far_part_copy(k).wait_recv()
        own = pl.ds(pl.multiple_of(side * cap, cap), cap)
        total = (
            part[k, mine].astype(jnp.float32)
            + near_part[k, own].astype(jnp.float32)
            + far_part[k].astype(jnp.float32)
        ).astype(jnp.bfloat16)

        @pl.when(k == 0)
        def _():
            ret_ref[k] = total

        @pl.when(k > 0)
        def _():
            result[k] = total
            return_copy(k).start()

    @pl.loop(0, ep + 2)
    def _(k):
        @pl.when(k + 1 < ep)
        def _():
            z_copy(k + 1).wait_recv()
            far_copy(k + 1).start()
            near_copy(k + 1).start()

        @pl.when(k < ep)
        def _():
            far_copy(k).wait_recv()
            relay_copy(k).start()

        @pl.when((k >= 1) & (k <= ep))
        def _():
            pair_stage(k - 1)

        @pl.when(k >= 2)
        def _():
            final_stage(k - 2)

        @pl.when(k == 0)
        def _():
            @pl.loop(0, tiles)
            def _(i):
                for copy in weight_copies(i):
                    copy.wait()

        @pl.when(k < ep)
        def _():
            near_copy(k).wait_recv()
            relay_copy(k).wait_recv()
            feed_forward(k)
            near_part_copy(k).start()

    @pl.loop(0, ep)
    def _(k):
        far_copy(k).wait_send()
        near_copy(k).wait_send()
        relay_copy(k).wait_send()
        near_part_copy(k).wait_send()
        far_part_copy(k).wait_send()

    @pl.loop(1, ep)
    def _(k):
        z_copy(k).wait_send()

        @pl.when(e + k < ep)
        def _():
            state_copy(k).wait_send()

        @pl.when(e >= k)
        def _():
            state_copy(k).wait_recv()

        return_copy(k).wait()


def expert_exchange(outgoing, state, gate, up, down):
    ep, tp = lax.axis_size("ep"), lax.axis_size("tp")
    _, cap, width = outgoing.shape
    part_hidden = gate.shape[2]
    tiles = part_hidden // LANES
    bf16 = jnp.bfloat16
    vmem = pl.BlockSpec(memory_space=pltpu.VMEM)
    hbm = pl.BlockSpec(memory_space=pl.ANY)
    pair = pltpu.SemaphoreType.DMA((2, ep))
    rows = ep * tp * cap
    return pl.pallas_call(
        functools.partial(expert_kernel, ep, tp, cap),
        out_shape=(
            jax.ShapeDtypeStruct(outgoing.shape, bf16),
            jax.ShapeDtypeStruct((ep,) + state.shape, jnp.float32),
        ),
        in_specs=[vmem, vmem, hbm, hbm, hbm],
        out_specs=(vmem, hbm),
        scratch_shapes=[
            pltpu.VMEM((tiles, width, 2 * LANES), bf16),
            pltpu.VMEM((part_hidden, width), bf16),
            pltpu.VMEM((ep, tp * cap, width), bf16),
            pltpu.VMEM((tp * cap, part_hidden), bf16),
            pltpu.VMEM((ep, tp * cap, width), bf16),
            pltpu.VMEM((ep, 2 * cap, width), bf16),
            pltpu.VMEM((ep, cap, width), bf16),
            pltpu.VMEM((ep, cap, width), bf16),
            pltpu.VMEM((ep, cap, width), bf16),
            pltpu.SemaphoreType.DMA((2, tiles)),
            pltpu.SemaphoreType.DMA((2,)),
        ]
        + [pair] * 8,
        compiler_params=pltpu.CompilerParams(
            collective_id=0, has_side_effects=True, vmem_limit_bytes=66000000
        ),
        cost_estimate=pl.CostEstimate(
            flops=6 * rows * width * part_hidden, bytes_accessed=6 * width * part_hidden,
            transcendentals=rows * part_hidden,
        ),
    )(outgoing, state, gate, up, down)


def pack_state(memory, normer, stabilizer, totals):
    heads = memory.shape[0]
    extra = jnp.concatenate(
        [
            normer[:, None, :],
            jnp.broadcast_to(stabilizer[:, None, None], (heads, 1, DH)),
            jnp.broadcast_to(totals[:, None, None], (heads, 1, DH)),
            jnp.zeros((heads, 5, DH), jnp.float32),
        ],
        axis=1,
    )
    return jnp.concatenate([memory, extra], axis=1)


def entering_state(states):
    place = lax.axis_index("ep")
    count = states.shape[0]
    turn = jnp.arange(count)
    valid = (turn >= 1) & (turn <= place)
    memory = jnp.where(valid[:, None, None, None], states[:, :, :DH], 0.0)
    normer = jnp.where(valid[:, None, None], states[:, :, DH], 0.0)
    stab = jnp.where(valid[:, None], states[:, :, DH + 1, 0], neg_big)
    totals = jnp.where(valid[:, None], states[:, :, DH + 2, 0], 0.0)
    nearer = turn[None, :] < turn[:, None]
    later = jnp.sum(jnp.where(nearer[:, :, None], totals[None], 0.0), axis=1)
    level = jnp.where(valid[:, None], stab + later, neg_big)
    stab_in = jnp.maximum(jnp.sum(totals, axis=0), jnp.max(level, axis=0))
    scale = jnp.where(valid[:, None], jnp.exp(level - stab_in[None]), 0.0)
    memory = jnp.sum(scale[:, :, None, None] * memory, axis=0)
    normer = jnp.sum(scale[:, :, None] * normer, axis=0)
    return memory, normer, stab_in


def state_update(state_in, inputs, cumulative):
    memory, normer, stabilizer = state_in
    key_rows, values, in_gate, forget = inputs
    block_total = cumulative[:, -1]
    weights = block_total[:, None] - cumulative + in_gate
    new_stab = jnp.maximum(block_total + stabilizer, jnp.max(weights, axis=-1))
    scaled = jnp.exp(weights - new_stab[:, None])
    retained = jnp.exp(block_total + stabilizer - new_stab)
    weighted_keys = scaled[:, :, None] * key_rows
    memory = retained[:, None, None] * memory + jnp.einsum(
        "hsd,hse->hde", weighted_keys, values, precision=highest
    )
    normer = retained[:, None] * normer + jnp.sum(weighted_keys, axis=1)
    return (memory, normer, new_stab)


def state_only(state_in, inputs):
    cumulative = jnp.cumsum(inputs[3], axis=-1)
    return (state_update(state_in, inputs, cumulative), None)


def block_step(state_in, inputs):
    memory, normer, stabilizer = state_in
    queries, key_rows, values, in_gate, forget = inputs
    length = queries.shape[1]
    causal = jnp.tril(jnp.ones((length, length), dtype=bool))
    cumulative = jnp.cumsum(forget, axis=-1)
    decays = jnp.where(
        causal, cumulative[:, :, None] - cumulative[:, None, :] + in_gate[:, None, :], -jnp.inf
    )
    carried_max = cumulative + stabilizer[:, None]
    row_max = jnp.maximum(jnp.max(decays, axis=-1), carried_max)
    scores = jnp.einsum("htd,hsd->hts", queries, key_rows, precision=highest) * jnp.exp(
        decays - row_max[:, :, None]
    )
    carried = jnp.exp(carried_max - row_max)
    numerator = carried[:, :, None] * jnp.einsum(
        "htd,hde->hte", queries, memory, precision=highest
    ) + jnp.einsum("hts,hse->hte", scores, values, precision=highest)
    denominator = carried * jnp.einsum("htd,hd->ht", queries, normer, precision=highest) + jnp.sum(
        scores, axis=-1
    )
    output = numerator / jnp.maximum(jnp.abs(denominator), jnp.exp(-row_max))[:, :, None]
    new_state = state_update(state_in, (key_rows, values, in_gate, forget), cumulative)
    return (new_state, output)


def split_blocks(row_block, heads):
    count = row_block.shape[0] // BLOCK
    return row_block.astype(jnp.float32).reshape(count, BLOCK, heads, -1).transpose(0, 2, 1, 3)


def gate_blocks(gate_rows):
    heads = gate_rows.shape[0]
    return gate_rows.reshape(heads, -1, BLOCK).transpose(1, 0, 2)


def route_slots(routing_expert_index, experts, stride):
    flat_ids = routing_expert_index.reshape(-1)
    onehot = (flat_ids[:, None] == jnp.arange(experts, dtype=jnp.int32)[None, :]).astype(jnp.int32)
    route_ranks = jnp.sum((jnp.cumsum(onehot, axis=0) - 1) * onehot, axis=1)
    turn = lax.rem(flat_ids + experts - lax.axis_index("ep"), experts)
    return (turn * stride + route_ranks).reshape(routing_expert_index.shape)


def on_device(
    memory_query_rows,
    memory_key_rows,
    memory_value_rows,
    input_gate_log,
    forget_gate_logits,
    forget_log_extra,
    memory_output_weight,
    second_batch_tokens,
    expert_norm_gain,
    routing_expert_index,
    routing_expert_weight,
    expert_gate_matrix,
    expert_up_matrix,
    expert_down_matrix,
):
    heads_local = input_gate_log.shape[0]
    positions = input_gate_log.shape[1]
    queries = split_blocks(memory_query_rows, heads_local)
    key_rows = split_blocks(memory_key_rows, heads_local) * DH ** (-0.5)
    values = split_blocks(memory_value_rows, heads_local)
    in_gate = gate_blocks(input_gate_log)
    forget_log_value = jax.nn.log_sigmoid(forget_gate_logits) + forget_log_extra
    forget = gate_blocks(forget_log_value)
    zero_memory = jnp.zeros((heads_local, DH, DH), jnp.float32)
    zero_normer = jnp.zeros((heads_local, DH), jnp.float32)
    low_stab = jnp.full((heads_local,), neg_big, jnp.float32)
    local_state, _ = lax.scan(
        state_only, (zero_memory, zero_normer, low_stab), (key_rows, values, in_gate, forget)
    )
    totals = jnp.sum(forget_log_value, axis=1)
    tok_rows = second_batch_tokens.shape[0]
    experts = lax.axis_size("ep")
    capacity = max(2, 5 * tok_rows * TOP // (4 * experts))
    stride = -(-capacity // 16) * 16
    slots_dev = experts * stride
    tokens_f = second_batch_tokens.astype(jnp.float32)
    normed = (
        tokens_f
        * lax.rsqrt(jnp.mean(tokens_f * tokens_f, axis=1, keepdims=True) + rms_eps)
        * expert_norm_gain
    ).astype(jnp.bfloat16)
    slot_ids = route_slots(routing_expert_index, experts, stride)
    slot_table = jnp.arange(slots_dev, dtype=jnp.int32)
    placing = jnp.zeros((slots_dev, tok_rows), jnp.bfloat16)
    for column in range(TOP):
        placing = placing + (slot_table[:, None] == slot_ids[None, :, column]).astype(jnp.bfloat16)
    outgoing = jnp.dot(placing, normed, preferred_element_type=jnp.float32).astype(jnp.bfloat16)
    returned, states = expert_exchange(
        outgoing.reshape(experts, stride, -1),
        pack_state(*local_state, totals),
        expert_gate_matrix,
        expert_up_matrix,
        expert_down_matrix,
    )
    incoming = entering_state(states)
    _, outputs = lax.scan(block_step, incoming, (queries, key_rows, values, in_gate, forget))
    memory_rows = outputs.transpose(0, 2, 1, 3).reshape(positions, -1).astype(jnp.bfloat16)
    mixed = jnp.dot(
        lax.all_gather(memory_rows, "tp", axis=1, tiled=True),
        memory_output_weight,
        preferred_element_type=jnp.float32,
    )
    mixed_out = mixed.astype(jnp.bfloat16)
    choosing = jnp.zeros((tok_rows, slots_dev), jnp.float32)
    for column in range(TOP):
        choosing = choosing + jnp.where(
            slot_table[None, :] == slot_ids[:, column : column + 1],
            routing_expert_weight[:, column : column + 1],
            0.0,
        )
    expert_out = jnp.dot(
        choosing, returned.reshape(slots_dev, -1).astype(jnp.float32), precision=highest
    ).astype(jnp.bfloat16)
    return (mixed_out, expert_out)


def solution(mesh):
    placed = (
        P(("grp", "ep"), "tp"),
        P(("grp", "ep"), "tp"),
        P(("grp", "ep"), "tp"),
        P("tp", ("grp", "ep")),
        P("tp", ("grp", "ep")),
        P("tp", ("grp", "ep")),
        P(None, "tp"),
        P(("grp", "ep", "tp"), None),
        P(),
        P(("grp", "ep", "tp"), None),
        P(("grp", "ep", "tp"), None),
        P("ep", None, "tp"),
        P("ep", None, "tp"),
        P("ep", "tp", None),
    )
    return jax.shard_map(
        on_device,
        mesh=mesh,
        in_specs=placed,
        out_specs=(P(("grp", "ep"), "tp"), P(("grp", "ep", "tp"), None)),
        check_vma=False,
    )
```

time: 222 us -> 139 us (0.63)
  Pallas kernels: 0 us -> 112 us
  blocking collectives: 87.7 us -> 5.78 us
  waiting for transfers between devices: 65.3 us -> 0 us
  matrix products: 31.6 us -> 5.84 us
  between operations: 15 us -> 0.85 us
  starting transfers between devices: 4.68 us -> 0 us
  local copies, waits for them, and re-layouts: 8.75 us -> 5.9 us
    pallas_call x0 -> x1, Pallas kernels: none -> 112 us  [expert_exchange(): pl.pallas_call(functools.partial(expert_kernel, ep, tp, cap), out_shape=(...]
    all_gather x1 -> x0, waiting for transfers between devices: 39.7 us -> none  [on_device(): row_block = lax.all_gather(arrived, 'tp', axis=0, tiled=True)]
    all_to_all x1 -> x0, blocking collectives: 37.6 us -> none  [on_device(): lax.all_to_all(outgoing, 'ep', split_axis=0, concat_axis=0, tiled=True)]
    all_gather x3 -> x0, blocking collectives: 35.8 us -> none  [entering(): gathered = jax.tree.map(lambda a: lax.all_gather(a, axis), part)]
    dot_general x2 -> x1, matrix products: 27.5 us -> 1.83 us  [on_device(): jnp.dot(choosing, returned.reshape(slots_dev, -1).astype(jnp.float32), pr...]
    all_to_all x1 -> x0, waiting for transfers between devices: 23 us -> none  [on_device(): lax.all_to_all(summed, 'ep', split_axis=0, concat_axis=0, tiled=True)]
    unnamed x1 -> x0, blocking collectives: 8.36 us -> none
    all_to_all x1 -> x0, starting transfers between devices: 4.6 us -> none  [on_device(): lax.all_to_all(summed, 'ep', split_axis=0, concat_axis=0, tiled=True)]
  transfers between devices with their start and end apart: 3 -> 0, of which waited for: 3 -> 0; matrix products, arithmetic and copies ran while one was open for 3% -> 0% of each run, Pallas kernels for 0% -> 0%
where the time goes in v1:
time: 139 us; the launch traced here: 138 us
  Pallas kernels  112 us (81%)
  other arithmetic  7.82 us (6%)
  local copies, waits for them, and re-layouts  5.9 us (4%)
  matrix products  5.84 us (4%)
  blocking collectives  5.78 us (4%)
    pallas_call x1, Pallas kernels, expert_exchange(): pl.pallas_call(functools.partial(expert_kernel, ep, tp, cap), out_shape=(...  112 us
    all_gather x1, blocking collectives, on_device(): lax.all_gather(memory_rows, 'tp', axis=1, tiled=True)  5.78 us

profile of v1, /device:TPU:0, one launch (start us, length us, event | category | flops | bytes accessed | tf_op | source)
XLA Modules:
  0.0 138.5 jit_solution(10617154768802616023)
XLA Ops:
  0.7 0.9 fusion.51
  1.5 0.3 reduce_window_sum.27
  1.8 0.2 slice_reduce_fusion
  2.0 0.9 fusion.53
  2.9 0.1 copy.138
  3.0 0.2 multiply_reduce_fusion.2
  3.3 0.9 convert_multiply_fusion.2
  4.2 1.0 copy.158
  5.2 0.4 convolution_add_fusion.1
  5.6 0.1 fusion.17
  5.7 0.1 broadcast_add_fusion
  5.9 1.3 concatenate.3.state_ref
  7.2 0.1 copy.133
  7.3 0.1 eq.86
  7.4 1.2 reduce-window.6
  8.7 0.1 slice.49
  8.7 0.1 copy.135
  8.9 0.1 copy.136
  9.0 0.1 add_bitcast_fusion
  9.1 0.1 eq.82
  9.2 0.1 reduce_sum.95
  9.5 0.2 fusion.4
  9.7 1.7 %convolution_convert_fusion = bf16[320,2048]{1,0:T(8,128)(2,1)} fusion(bf16[128,2048]{1,0:T(8,128)(2,1)S(1)} %copy-done, f32[2048]{0:T(1024)S(1)} %copy-done.4, f32[128]{0:T(128)S(1)} %add_rsqrt_fusion, s32[128]{0:T(128)S(1)} %get-tuple-element.77, s32[128]{0:T(128)S(1)} %get-tuple-element.76), kind=kOutput, calls=%fused_computation | convolution fusion | flops 169803776 | bytes 1844736 | tf_op jit(solution)/shard_map/dot_general | solution.py:447
  11.3 112.3 %shard_map.149 = (bf16[4,80,2048]{2,1,0:T(8,128)(2,1)}, f32[4,2,136,128]{3,2,1,0:T(8,128)}) custom-call(bf16[4,80,2048]{2,1,0:T(8,128)(2,1)} %bitcast.95, f32[2,136,128]{2,1,0:T(8,128)} %concatenate.3.state_ref, bf16[1,2048,896]{2,1,0:T(8,128)(2,1)} %gate_hbm.1, bf16[1,2048,896]{2,1,0:T(8,128)(2,1)} %up_hbm.1, bf16[1,896,2048]{2,1,0:T(8,128)(2,1)} %down_hbm.1), custom_call_target="tpu_custom_call" | custom-call | flops 14092861440 | bytes 11010048 | tf_op jit(solution)/shard_map/pallas_call | solution.py:270
  123.7 0.9 fusion.54
  124.5 0.1 copy.143
  124.6 0.1 fusion.50
  124.8 0.1 select_reduce_fusion
  124.9 0.1 copy.144
  125.0 0.1 fusion.49
  125.1 0.1 exponential_select_fusion
  125.2 0.1 copy.151
  125.3 0.8 slice.46
  126.0 0.1 multiply_reduce_fusion.1
  126.1 0.2 fusion.30
  126.4 0.1 fusion.16
  126.6 0.3 fusion.55
  126.9 0.1 exponential_maximum_fusion
  127.0 0.1 copy.145
  127.1 0.8 broadcast_select_fusion
  127.9 0.1 copy.146
  128.0 0.1 copy.147
  128.1 1.2 multiply_reduce_fusion
  129.3 0.3 fusion.1
  129.6 0.2 fusion.3
  129.9 5.8 %all_gather.3 = bf16[128,1024]{0,1:T(8,128)(2,1)S(1)} all-gather(bf16[128,256]{0,1:T(8,128)(2,1)S(1)} %bitcast.98), channel_id=1, replica_groups=mesh['grp'=2,'ep'=4,'tp'=4] {'tp'}, dimensions={1}, use_global_device_ids=true | all-gather | bytes 327680 | tf_op jit(solution)/shard_map/all_gather | solution.py:459
  135.6 1.0 convolution_convert_fusion.2
  136.7 1.8 %convolution_convert_fusion.1 = bf16[128,2048]{1,0:T(8,128)(2,1)} fusion(bf16[320,2048]{1,0:T(8,128)(2,1)S(1)} %bitcast.94, f32[128]{0:T(128)S(1)} %get-tuple-element.73, s32[128]{0:T(128)S(1)} %get-tuple-element.77, f32[128]{0:T(128)S(1)} %get-tuple-element.72, s32[128]{0:T(128)S(1)} %get-tuple-element.76), kind=kOutput, calls=%fused_computation.1 | convolution fusion | flops 1007099904 | bytes 1837056 | tf_op jit(solution)/shard_map/dot_general | solution.py:471
  (37 shorter events, 0.6 us)
Async XLA Ops:
  0.6 6.5 %copy-start.5 = (s32[128,2]{0,1:T(2,128)S(1)}, s32[128,2]{0,1:T(2,128)}, u32[]{:S(2)}) copy-start(s32[128,2]{0,1:T(2,128)} %param.23) | copy-start | bytes 3076
  0.6 8.8 %copy-start = (bf16[128,2048]{1,0:T(8,128)(2,1)S(1)}, bf16[128,2048]{1,0:T(8,128)(2,1)}, u32[]{:S(2)}) copy-start(bf16[128,2048]{1,0:T(8,128)(2,1)} %param.21) | copy-start | bytes 1572868
  0.7 9.0 %copy-start.4 = (f32[2048]{0:T(1024)S(1)}, f32[2048]{0:T(1024)}, u32[]{:S(2)}) copy-start(f32[2048]{0:T(1024)} %param.22) | copy-start | bytes 24580
  11.3 114.8 %copy-start.3 = (bf16[128,256]{1,0:T(8,128)(2,1)S(1)}, bf16[128,256]{1,0:T(8,128)(2,1)}, u32[]{:S(2)}) copy-start(bf16[128,256]{1,0:T(8,128)(2,1)} %param.14) | copy-start | bytes 196612
  11.3 115.0 %copy-start.6 = (f32[2,128]{1,0:T(2,128)S(1)}, f32[2,128]{1,0:T(2,128)}, u32[]{:S(2)}) copy-start(f32[2,128]{1,0:T(2,128)} %param.17) | copy-start | bytes 3076
  123.6 12.0 %copy-start.2 = (bf16[1024,512]{1,0:T(8,128)(2,1)S(1)}, bf16[1024,512]{1,0:T(8,128)(2,1)}, u32[]{:S(2)}) copy-start(bf16[1024,512]{1,0:T(8,128)(2,1)} %param.20) | copy-start | bytes 3145732
  129.3 7.3 %copy-start.7 = (f32[128,2]{0,1:T(2,128)S(1)}, f32[128,2]{0,1:T(2,128)}, u32[]{:S(2)}) copy-start(f32[128,2]{0,1:T(2,128)} %param.24) | copy-start | bytes 3076
  129.3 7.3 %copy-start.1 = (bf16[4,80,2048]{2,1,0:T(8,128)(2,1)S(1)}, bf16[4,80,2048]{2,1,0:T(8,128)(2,1)}, u32[]{:S(2)}) copy-start(bf16[4,80,2048]{2,1,0:T(8,128)(2,1)} %get-tuple-element.39) | copy-start | bytes 3932164

commit v2 on v1

v2 whole, which is shorter than its diff:
```python
import functools

import jax
import jax.numpy as jnp
from jax import lax
from jax.experimental import pallas as pl
from jax.experimental.pallas import tpu as pltpu
from jax.sharding import PartitionSpec as P

DH = 128
TOP = 2
BLOCK = 128


neg_big = -1e30
rms_eps = 1e-06
highest = lax.Precision.HIGHEST


MESH = pl.DeviceIdType.MESH
LANES = 128


def expert_kernel(
    ep,
    tp,
    cap,
    out_ref,
    query_ref,
    key_ref,
    value_ref,
    in_gate_ref,
    logit_ref,
    extra_ref,
    mix_hbm,
    gate_hbm,
    up_hbm,
    down_hbm,
    ret_ref,
    mixed_ref,
    gate_up,
    down,
    rows,
    hidden,
    part,
    near_part,
    pair_sum,
    far_part,
    result,
    local_state,
    state_in,
    state_out,
    memory,
    mix,
    w_sem,
    own_sem,
    st_sem,
    z_sem,
    far_sem,
    near_sem,
    relay_sem,
    np_sem,
    fp_sem,
    r_sem,
    m_sem,
):
    e = lax.axis_index("ep")
    t = lax.axis_index("tp")
    side, core = t // 2, t % 2
    near = side * 2 + (1 - core)
    far = (1 - side) * 2 + core
    across = (1 - side) * 2 + (1 - core)
    heads = in_gate_ref.shape[0]
    length = in_gate_ref.shape[1]
    tiles = gate_up.shape[0]
    width = rows.shape[2]

    def place(side_at, core_at):
        return pl.ds(pl.multiple_of((core_at * 2 + side_at) * cap, cap), cap)

    mine = place(side, core)
    theirs = place(1 - side, core)

    def remote(src, dst, sems, k, target):
        return pltpu.make_async_remote_copy(
            src_ref=src,
            dst_ref=dst,
            send_sem=sems.at[0, k],
            recv_sem=sems.at[1, k],
            device_id=target,
            device_id_type=MESH,
        )

    def ahead(k):
        return {"ep": lax.rem(e + k, ep)}

    def behind(k):
        return {"ep": lax.rem(e + ep - k, ep)}

    def weight_copies(i):
        cols = pl.ds(pl.multiple_of(i * LANES, LANES), LANES)
        return (
            pltpu.make_async_copy(
                gate_hbm.at[0, :, cols], gate_up.at[i, :, pl.ds(0, LANES)], w_sem.at[0, i]
            ),
            pltpu.make_async_copy(
                up_hbm.at[0, :, cols], gate_up.at[i, :, pl.ds(LANES, LANES)], w_sem.at[1, i]
            ),
        )

    down_copy = pltpu.make_async_copy(down_hbm.at[0], down, own_sem.at[1])
    own_copy = pltpu.make_async_copy(out_ref.at[0], rows.at[0, mine], own_sem.at[0])

    def z_copy(k):
        return remote(out_ref.at[k], rows.at[k, mine], z_sem, k, ahead(k))

    state_copy = remote(state_out, state_in, st_sem, 0, ahead(1))
    mix_copy = pltpu.make_async_copy(mix_hbm, mix, own_sem.at[2])

    def memory_copy(i):
        span = memory.at[t]
        return remote(span, span, m_sem, i, {"tp": (near, far, across)[i]})

    def gates(h):
        logits = logit_ref[h : h + 1, :]
        forget = (
            jnp.minimum(logits, 0.0) - jnp.log1p(jnp.exp(-jnp.abs(logits)))
        ) + extra_ref[h : h + 1, :]
        at_row = lax.broadcasted_iota(jnp.int32, (length, length), 0)
        at_col = lax.broadcasted_iota(jnp.int32, (length, length), 1)
        diagonal = at_row == at_col
        in_row = in_gate_ref[h : h + 1, :]
        in_col = jnp.sum(jnp.where(diagonal, in_row, 0.0), axis=1, keepdims=True)
        sum_col = jnp.sum(jnp.where(at_col <= at_row, forget, 0.0), axis=1, keepdims=True)
        sum_row = jnp.sum(jnp.where(diagonal, sum_col, 0.0), axis=0, keepdims=True)
        total = jnp.sum(forget, axis=1, keepdims=True)
        return in_row, in_col, sum_row, sum_col, total, at_col <= at_row

    def head(ref, h):
        return ref[:, h * DH : (h + 1) * DH].astype(jnp.float32)

    def local_part():
        for h in range(heads):
            _, in_col, _, sum_col, total, _ = gates(h)
            weights = total - sum_col + in_col
            stab = jnp.max(weights, axis=0, keepdims=True)
            weighted = jnp.exp(weights - stab) * (head(key_ref, h) * DH ** (-0.5))
            local_state[h, 0:DH, :] = jnp.dot(
                weighted.T, head(value_ref, h), precision=highest,
                preferred_element_type=jnp.float32,
            )
            local_state[h, DH : DH + 1, :] = jnp.sum(weighted, axis=0, keepdims=True)
            local_state[h, DH + 1 : DH + 2, :] = jnp.broadcast_to(stab, (1, DH))
            local_state[h, DH + 2 : DH + 3, :] = jnp.broadcast_to(total, (1, DH))

    def pass_state():
        for h in range(heads):
            total = local_state[h, DH + 2 : DH + 3, :]
            stab_own = local_state[h, DH + 1 : DH + 2, :]
            carried = total + state_in[h, DH + 1 : DH + 2, :]
            stab = jnp.maximum(carried, stab_own)
            old, new = jnp.exp(carried - stab), jnp.exp(stab_own - stab)
            state_out[h, 0 : DH + 1, :] = (
                old * state_in[h, 0 : DH + 1, :] + new * local_state[h, 0 : DH + 1, :]
            )
            state_out[h, DH + 1 : DH + 2, :] = stab
        state_copy.start()

    def memory_part():
        for h in range(heads):
            in_row, _, sum_row, sum_col, _, causal = gates(h)
            decays = jnp.where(causal, sum_col - sum_row + in_row, -jnp.inf)
            carried_max = sum_col + state_in[h, DH + 1 : DH + 2, 0:1]
            row_max = jnp.maximum(jnp.max(decays, axis=1, keepdims=True), carried_max)
            queries = head(query_ref, h)
            keys = head(key_ref, h) * DH ** (-0.5)
            scores = jnp.dot(
                queries, keys.T, precision=highest, preferred_element_type=jnp.float32
            ) * jnp.exp(decays - row_max)
            carried = jnp.exp(carried_max - row_max)
            numerator = carried * jnp.dot(
                queries, state_in[h, 0:DH, :], precision=highest,
                preferred_element_type=jnp.float32,
            ) + jnp.dot(
                scores, head(value_ref, h), precision=highest,
                preferred_element_type=jnp.float32,
            )
            denominator = carried * jnp.sum(
                queries * state_in[h, DH : DH + 1, :], axis=1, keepdims=True
            ) + jnp.sum(scores, axis=1, keepdims=True)
            memory[t, :, h * DH : (h + 1) * DH] = (
                numerator / jnp.maximum(jnp.abs(denominator), jnp.exp(-row_max))
            ).astype(jnp.bfloat16)
        for i in range(3):
            memory_copy(i).start()

    def mix_part():
        mix_copy.wait()
        for i in range(3):
            memory_copy(i).wait_recv()
        total = jnp.zeros(mixed_ref.shape, jnp.float32)
        for i in range(tp):
            total = total + jnp.dot(
                memory[i], mix[i * heads * DH : (i + 1) * heads * DH, :],
                preferred_element_type=jnp.float32,
            )
        mixed_ref[...] = total.astype(jnp.bfloat16)

    def far_copy(k):
        return remote(rows.at[k, mine], rows.at[k, mine], far_sem, k, {"tp": far})

    def near_copy(k):
        return remote(rows.at[k, mine], rows.at[k, mine], near_sem, k, {"tp": near})

    def relay_copy(k):
        return remote(rows.at[k, theirs], rows.at[k, theirs], relay_sem, k, {"tp": near})

    def near_part_copy(k):
        span = pl.ds(pl.multiple_of((1 - core) * 2 * cap, 2 * cap), 2 * cap)
        return remote(part.at[k, span], near_part.at[k], np_sem, k, {"tp": near})

    def far_part_copy(k):
        return remote(pair_sum.at[k], far_part.at[k], fp_sem, k, {"tp": far})

    def return_copy(k):
        return remote(result.at[k], ret_ref.at[k], r_sem, k, behind(k))

    barrier = pltpu.get_barrier_semaphore()

    @pl.loop(1, ep)
    def _(k):
        pl.semaphore_signal(barrier, inc=1, device_id=ahead(k), device_id_type=MESH)

    for target in (near, far, across):
        pl.semaphore_signal(barrier, inc=1, device_id={"tp": target}, device_id_type=MESH)
    own_copy.start()
    pl.semaphore_wait(barrier, ep + 2)

    @pl.when(ep > 1)
    def _():
        z_copy(1).start()

    own_copy.wait()
    far_copy(0).start()
    near_copy(0).start()

    @pl.loop(0, tiles)
    def _(i):
        for copy in weight_copies(i):
            copy.start()

    down_copy.start()
    mix_copy.start()
    local_part()

    @pl.when(e == 0)
    def _():
        state_in[...] = jnp.zeros_like(state_in)
        if ep > 1:
            pass_state()

    def feed_forward(k):
        @pl.loop(0, tiles)
        def _(i):
            both = jnp.dot(rows[k], gate_up[i], preferred_element_type=jnp.float32)
            act, up_act = both[:, :LANES], both[:, LANES:]
            hidden[:, pl.ds(pl.multiple_of(i * LANES, LANES), LANES)] = (
                jax.nn.silu(act) * up_act
            ).astype(jnp.bfloat16)

        @pl.when(k == 0)
        def _():
            down_copy.wait()

        @pl.loop(0, width // 256)
        def _(i):
            cols = pl.ds(pl.multiple_of(i * 256, 256), 256)
            part[k, :, cols] = jnp.dot(
                hidden[...], down[:, cols], preferred_element_type=jnp.float32
            ).astype(jnp.bfloat16)

    def pair_stage(k):
        near_part_copy(k).wait_recv()
        other = pl.ds(pl.multiple_of((1 - side) * cap, cap), cap)
        pair_sum[k] = (
            part[k, theirs].astype(jnp.float32) + near_part[k, other].astype(jnp.float32)
        ).astype(jnp.bfloat16)
        far_part_copy(k).start()

    def final_stage(k):
        far_part_copy(k).wait_recv()
        own = pl.ds(pl.multiple_of(side * cap, cap), cap)
        total = (
            part[k, mine].astype(jnp.float32)
            + near_part[k, own].astype(jnp.float32)
            + far_part[k].astype(jnp.float32)
        ).astype(jnp.bfloat16)

        @pl.when(k == 0)
        def _():
            ret_ref[k] = total

        @pl.when(k > 0)
        def _():
            result[k] = total
            return_copy(k).start()

    @pl.loop(0, ep + 1)
    def _(k):
        @pl.when(k >= 1)
        def _():
            pair_stage(k - 1)

        @pl.when(k < ep)
        def _():
            far_copy(k).wait_recv()
            relay_copy(k).start()

        @pl.when(k + 1 < ep)
        def _():
            z_copy(k + 1).wait_recv()
            far_copy(k + 1).start()
            near_copy(k + 1).start()

        @pl.when(k + 2 < ep)
        def _():
            z_copy(k + 2).start()

        @pl.when(k == 0)
        def _():
            @pl.loop(0, tiles)
            def _(i):
                for copy in weight_copies(i):
                    copy.wait()

        @pl.when(k < ep)
        def _():
            near_copy(k).wait_recv()
            relay_copy(k).wait_recv()
            feed_forward(k)
            near_part_copy(k).start()

        @pl.when((k > 0) & (e == k))
        def _():
            state_copy.wait_recv()

            @pl.when(e + 1 < ep)
            def _():
                pass_state()

        @pl.when((k < ep) & (e == k))
        def _():
            memory_part()

        @pl.when(k >= 1)
        def _():
            final_stage(k - 1)

    mix_part()
    for i in range(3):
        memory_copy(i).wait_send()

    @pl.when(e + 1 < ep)
    def _():
        state_copy.wait_send()

    @pl.loop(0, ep)
    def _(k):
        far_copy(k).wait_send()
        near_copy(k).wait_send()
        relay_copy(k).wait_send()
        near_part_copy(k).wait_send()
        far_part_copy(k).wait_send()

    @pl.loop(1, ep)
    def _(k):
        z_copy(k).wait_send()

        return_copy(k).wait()


def expert_exchange(outgoing, memory_args, mix_weight, gate, up, down):
    ep, tp = lax.axis_size("ep"), lax.axis_size("tp")
    _, cap, width = outgoing.shape
    part_hidden = gate.shape[2]
    tiles = part_hidden // LANES
    bf16 = jnp.bfloat16
    vmem = pl.BlockSpec(memory_space=pltpu.VMEM)
    hbm = pl.BlockSpec(memory_space=pl.ANY)
    pair = pltpu.SemaphoreType.DMA((2, ep))
    rows = ep * tp * cap
    positions = memory_args[0].shape[0]
    heads = memory_args[3].shape[0]
    state = pltpu.VMEM((heads, DH + 8, DH), jnp.float32)
    return pl.pallas_call(
        functools.partial(expert_kernel, ep, tp, cap),
        out_shape=(
            jax.ShapeDtypeStruct(outgoing.shape, bf16),
            jax.ShapeDtypeStruct((positions, mix_weight.shape[1]), bf16),
        ),
        in_specs=[vmem] * 7 + [hbm] * 4,
        out_specs=(vmem, vmem),
        scratch_shapes=[
            pltpu.VMEM((tiles, width, 2 * LANES), bf16),
            pltpu.VMEM((part_hidden, width), bf16),
            pltpu.VMEM((ep, tp * cap, width), bf16),
            pltpu.VMEM((tp * cap, part_hidden), bf16),
            pltpu.VMEM((ep, tp * cap, width), bf16),
            pltpu.VMEM((ep, 2 * cap, width), bf16),
            pltpu.VMEM((ep, cap, width), bf16),
            pltpu.VMEM((ep, cap, width), bf16),
            pltpu.VMEM((ep, cap, width), bf16),
            state,
            state,
            state,
            pltpu.VMEM((tp, positions, heads * DH), bf16),
            pltpu.VMEM(mix_weight.shape, bf16),
            pltpu.SemaphoreType.DMA((2, tiles)),
            pltpu.SemaphoreType.DMA((3,)),
        ]
        + [pair] * 8
        + [pltpu.SemaphoreType.DMA((2, 3))],
        compiler_params=pltpu.CompilerParams(
            collective_id=0, has_side_effects=True, vmem_limit_bytes=66000000
        ),
        cost_estimate=pl.CostEstimate(
            flops=6 * rows * width * part_hidden, bytes_accessed=6 * width * part_hidden,
            transcendentals=rows * part_hidden,
        ),
    )(outgoing, *memory_args, mix_weight, gate, up, down)


def route_slots(routing_expert_index, experts, stride):
    flat_ids = routing_expert_index.reshape(-1)
    onehot = (flat_ids[:, None] == jnp.arange(experts, dtype=jnp.int32)[None, :]).astype(jnp.int32)
    route_ranks = jnp.sum((jnp.cumsum(onehot, axis=0) - 1) * onehot, axis=1)
    turn = lax.rem(flat_ids + experts - lax.axis_index("ep"), experts)
    return (turn * stride + route_ranks).reshape(routing_expert_index.shape)


def on_device(
    memory_query_rows,
    memory_key_rows,
    memory_value_rows,
    input_gate_log,
    forget_gate_logits,
    forget_log_extra,
    memory_output_weight,
    second_batch_tokens,
    expert_norm_gain,
    routing_expert_index,
    routing_expert_weight,
    expert_gate_matrix,
    expert_up_matrix,
    expert_down_matrix,
):
    tok_rows = second_batch_tokens.shape[0]
    experts = lax.axis_size("ep")
    capacity = max(2, 5 * tok_rows * TOP // (4 * experts))
    stride = -(-capacity // 16) * 16
    slots_dev = experts * stride
    tokens_f = second_batch_tokens.astype(jnp.float32)
    normed = (
        tokens_f
        * lax.rsqrt(jnp.mean(tokens_f * tokens_f, axis=1, keepdims=True) + rms_eps)
        * expert_norm_gain
    ).astype(jnp.bfloat16)
    slot_ids = route_slots(routing_expert_index, experts, stride)
    slot_table = jnp.arange(slots_dev, dtype=jnp.int32)
    placing = jnp.zeros((slots_dev, tok_rows), jnp.bfloat16)
    for column in range(TOP):
        placing = placing + (slot_table[:, None] == slot_ids[None, :, column]).astype(jnp.bfloat16)
    outgoing = jnp.dot(placing, normed, preferred_element_type=jnp.float32).astype(jnp.bfloat16)
    returned, mixed_out = expert_exchange(
        outgoing.reshape(experts, stride, -1),
        (
            memory_query_rows,
            memory_key_rows,
            memory_value_rows,
            input_gate_log,
            forget_gate_logits,
            forget_log_extra,
        ),
        memory_output_weight,
        expert_gate_matrix,
        expert_up_matrix,
        expert_down_matrix,
    )
    choosing = jnp.zeros((tok_rows, slots_dev), jnp.float32)
    for column in range(TOP):
        choosing = choosing + jnp.where(
            slot_table[None, :] == slot_ids[:, column : column + 1],
            routing_expert_weight[:, column : column + 1],
            0.0,
        )
    expert_out = jnp.dot(
        choosing, returned.reshape(slots_dev, -1).astype(jnp.float32), precision=highest
    ).astype(jnp.bfloat16)
    return (mixed_out, expert_out)


def solution(mesh):
    placed = (
        P(("grp", "ep"), "tp"),
        P(("grp", "ep"), "tp"),
        P(("grp", "ep"), "tp"),
        P("tp", ("grp", "ep")),
        P("tp", ("grp", "ep")),
        P("tp", ("grp", "ep")),
        P(None, "tp"),
        P(("grp", "ep", "tp"), None),
        P(),
        P(("grp", "ep", "tp"), None),
        P(("grp", "ep", "tp"), None),
        P("ep", None, "tp"),
        P("ep", None, "tp"),
        P("ep", "tp", None),
    )
    return jax.shard_map(
        on_device,
        mesh=mesh,
        in_specs=placed,
        out_specs=(P(("grp", "ep"), "tp"), P(("grp", "ep", "tp"), None)),
        check_vma=False,
    )
```

time: 139 us -> 101 us (0.73)
  Pallas kernels: 112 us -> 88.4 us
  blocking collectives: 5.78 us -> 0 us
  other arithmetic: 7.82 us -> 3.31 us
  local copies, waits for them, and re-layouts: 5.9 us -> 2.22 us
    pallas_call x1, Pallas kernels: 112 us -> 88.4 us  [expert_exchange(): pl.pallas_call(functools.partial(expert_kernel, ep, tp, cap), out_shape=(...]
    all_gather x1 -> x0, blocking collectives: 5.78 us -> none  [on_device(): lax.all_gather(memory_rows, 'tp', axis=1, tiled=True)]
    reduce_sum x6 -> x0, other arithmetic: 2.45 us -> none  [the longest x1 1.17 us: entering_state(): memory = jnp.sum(scale[:, :, None, None] * memory, axis=0)]
    dot_general x6 -> x0, matrix products: 2.35 us -> none  [the longest x1 1.01 us: on_device(): jnp.dot(lax.all_gather(memory_rows, 'tp', axis=1, tiled=True), memory_out...]
    slice x5 -> x2, local copies, waits for them, and re-layouts: 2.03 us -> 0.18 us  [the longest x2 0.97 us: entering_state(): stab = jnp.where(valid[:, None], states[:, :, DH + 1, 0], neg_big)]
where the time goes in v2:
time: 101 us
  Pallas kernels  88.4 us (88%)
  matrix products  5.89 us (6%)
  other arithmetic  3.31 us (3%)
  local copies, waits for them, and re-layouts  2.22 us (2%)
    pallas_call x1, Pallas kernels, expert_exchange(): pl.pallas_call(functools.partial(expert_kernel, ep, tp, cap), out_shape=(...  88.4 us
    dot_general x1, matrix products, on_device(): jnp.dot(choosing, returned.reshape(slots_dev, -1).astype(jnp.float32), pr...  3.18 us
    dot_general x1, matrix products, on_device(): jnp.dot(placing, normed, preferred_element_type=jnp.float32)  2.7 us

profile of v2, /device:TPU:0, one launch (start us, length us, event | category | flops | bytes accessed | tf_op | source)
XLA Modules:
  0.0 100.5 jit_solution(18148060720118287590)
XLA Ops:
  0.6 0.8 copy.40
  1.4 0.1 eq.86
  1.6 1.2 %reduce-window.6 = s32[4,2,128]{2,1,0:T(2,128)S(1)} reduce-window(s32[4,2,128]{2,1,0:T(2,128)S(1)} %compare_convert_fusion, s32[]{:T(128)} %constant.21.clone.1), window={size=1x1x128 pad=0_0x0_0x127_0}, to_apply=%region_0.0 | reduce-window | flops 130048 | bytes 8196 | tf_op jit(solution)/shard_map/reduce-window
  2.8 0.1 slice.26
  2.9 0.1 copy.42
  3.0 0.1 copy.43
  3.1 0.1 add_bitcast_fusion
  3.2 0.1 eq.82
  3.4 0.1 reduce_sum.21
  3.5 0.1 copy.44
  3.6 0.7 fusion.25
  4.3 1.2 %fusion = f32[128]{0:T(128)S(1)} fusion(bf16[128,2048]{1,0:T(8,128)(2,1)} %param.21), kind=kLoop, calls=%fused_computation.4 | loop fusion | flops 786304 | bytes 524800 | tf_op jit(solution)/shard_map/reduce_sum | solution.py:465
  5.5 2.7 %convolution_convert_fusion = bf16[320,2048]{1,0:T(8,128)(2,1)} fusion(bf16[128,2048]{1,0:T(8,128)(2,1)} %param.21, f32[2048]{0:T(1024)} %param.22, f32[128]{0:T(128)S(1)} %add_rsqrt_fusion, s32[128]{0:T(128)S(1)} %get-tuple-element.9, s32[128]{0:T(128)S(1)} %get-tuple-element.8), kind=kOutput, calls=%fused_computation | convolution fusion | flops 169803776 | bytes 1844736 | tf_op jit(solution)/shard_map/dot_general | solution.py:473
  8.2 0.0 copy-start.1
  8.2 88.4 %shard_map.149 = (bf16[4,80,2048]{2,1,0:T(8,128)(2,1)}, bf16[128,512]{1,0:T(8,128)(2,1)}) custom-call(bf16[4,80,2048]{2,1,0:T(8,128)(2,1)} %bitcast.27, bf16[128,256]{1,0:T(8,128)(2,1)} %query_ref.1, bf16[128,256]{1,0:T(8,128)(2,1)} %key_ref.1, bf16[128,256]{1,0:T(8,128)(2,1)} %value_ref.1, f32[2,128]{1,0:T(2,128)} %in_gate_ref.1, f32[2,128]{1,0:T(2,128)} %logit_ref.1, ...), custom_call_target="tpu_custom_call" | custom-call | flops 14092861440 | bytes 11010048 | tf_op jit(solution)/shard_map/pallas_call | solution.py:395
  96.6 0.0 copy-start
  96.6 0.0 copy-done.1
  96.7 3.2 %convolution_convert_fusion.1 = bf16[128,2048]{1,0:T(8,128)(2,1)} fusion(bf16[320,2048]{1,0:T(8,128)(2,1)} %bitcast.26, f32[128]{0:T(128)S(1)} %get-tuple-element.7, s32[128]{0:T(128)S(1)} %get-tuple-element.9, f32[128]{0:T(128)S(1)} %get-tuple-element.6, s32[128]{0:T(128)S(1)} %get-tuple-element.8), kind=kOutput, calls=%fused_computation.1 | convolution fusion | flops 1007099904 | bytes 1837056 | tf_op jit(solution)/shard_map/dot_general | solution.py:496
  99.9 0.0 copy-done
  99.9 0.7 copy.48
  (7 shorter events, 0.1 us)
Async XLA Ops:
  8.2 88.4 %copy-start.1 = (f32[128,2]{0,1:T(2,128)S(1)}, f32[128,2]{0,1:T(2,128)}, u32[]{:S(2)}) copy-start(f32[128,2]{0,1:T(2,128)} %param.24) | copy-start | bytes 3076
  96.6 3.2 %copy-start = (bf16[128,512]{1,0:T(8,128)(2,1)S(1)}, bf16[128,512]{1,0:T(8,128)(2,1)}, u32[]{:S(2)}) copy-start(bf16[128,512]{1,0:T(8,128)(2,1)} %get-tuple-element.12) | copy-start | bytes 393220

commit v3 on v2

--- a/solution.py
+++ b/solution.py
@@ -432,8 +432,9 @@
 
 def route_slots(routing_expert_index, experts, stride):
     flat_ids = routing_expert_index.reshape(-1)
-    onehot = (flat_ids[:, None] == jnp.arange(experts, dtype=jnp.int32)[None, :]).astype(jnp.int32)
-    route_ranks = jnp.sum((jnp.cumsum(onehot, axis=0) - 1) * onehot, axis=1)
+    order = jnp.arange(flat_ids.shape[0], dtype=jnp.int32)
+    earlier = (flat_ids[:, None] == flat_ids[None, :]) & (order[None, :] < order[:, None])
+    route_ranks = jnp.sum(earlier.astype(jnp.int32), axis=1)
     turn = lax.rem(flat_ids + experts - lax.axis_index("ep"), experts)
     return (turn * stride + route_ranks).reshape(routing_expert_index.shape)
 
@@ -494,7 +495,7 @@
             0.0,
         )
     expert_out = jnp.dot(
-        choosing, returned.reshape(slots_dev, -1).astype(jnp.float32), precision=highest
+        choosing, returned.reshape(slots_dev, -1).astype(jnp.float32), precision=lax.Precision.HIGH
     ).astype(jnp.bfloat16)
     return (mixed_out, expert_out)
 

time: 101 us -> 98.9 us (0.979)
  other arithmetic: 3.31 us -> 2.13 us
    another operation x2 -> x0, other arithmetic: 1.26 us -> none
where the time goes in v3:
time: 98.9 us; the launch traced here: 98.6 us
  Pallas kernels  88.4 us (89%)
  matrix products  5.61 us (6%)
  other arithmetic  2.13 us (2%)
  local copies, waits for them, and re-layouts  1.8 us (2%)
    pallas_call x1, Pallas kernels, expert_exchange(): pl.pallas_call(functools.partial(expert_kernel, ep, tp, cap), out_shape=(...  88.4 us
    dot_general x1, matrix products, on_device(): jnp.dot(choosing, returned.reshape(slots_dev, -1).astype(jnp.float32), pr...  2.91 us
    dot_general x1, matrix products, on_device(): jnp.dot(placing, normed, preferred_element_type=jnp.float32)  2.7 us

profile of v3, /device:TPU:0, one launch (start us, length us, event | category | flops | bytes accessed | tf_op | source)
XLA Modules:
  0.0 98.6 jit_solution(15202046631747589183)
XLA Ops:
  0.6 0.8 copy.40
  1.4 0.1 eq.72
  1.6 0.2 convert_reduce_fusion
  1.7 0.1 reduce_sum.21
  1.9 0.1 copy.41
  2.0 0.7 fusion.24
  2.7 1.2 %fusion = f32[128]{0:T(128)S(1)} fusion(bf16[128,2048]{1,0:T(8,128)(2,1)} %param.21), kind=kLoop, calls=%fused_computation.4 | loop fusion | flops 786304 | bytes 524800 | tf_op jit(solution)/shard_map/reduce_sum | solution.py:466
  3.9 2.7 %convolution_convert_fusion = bf16[320,2048]{1,0:T(8,128)(2,1)} fusion(bf16[128,2048]{1,0:T(8,128)(2,1)} %param.21, f32[2048]{0:T(1024)} %param.22, f32[128]{0:T(128)S(1)} %add_rsqrt_fusion, s32[128]{0:T(128)S(1)} %get-tuple-element.9, s32[128]{0:T(128)S(1)} %get-tuple-element.8), kind=kOutput, calls=%fused_computation | convolution fusion | flops 169803776 | bytes 1844736 | tf_op jit(solution)/shard_map/dot_general | solution.py:474
  6.6 0.0 copy-start.1
  6.6 88.4 %shard_map.149 = (bf16[4,80,2048]{2,1,0:T(8,128)(2,1)}, bf16[128,512]{1,0:T(8,128)(2,1)}) custom-call(bf16[4,80,2048]{2,1,0:T(8,128)(2,1)} %bitcast.12, bf16[128,256]{1,0:T(8,128)(2,1)} %query_ref.1, bf16[128,256]{1,0:T(8,128)(2,1)} %key_ref.1, bf16[128,256]{1,0:T(8,128)(2,1)} %value_ref.1, f32[2,128]{1,0:T(2,128)} %in_gate_ref.1, f32[2,128]{1,0:T(2,128)} %logit_ref.1, ...), custom_call_target="tpu_custom_call" | custom-call | flops 14092861440 | bytes 11010048 | tf_op jit(solution)/shard_map/pallas_call | solution.py:395
  95.0 0.0 copy-start
  95.0 0.0 copy-done.1
  95.1 2.9 %convolution_convert_fusion.1 = bf16[128,2048]{1,0:T(8,128)(2,1)} fusion(bf16[320,2048]{1,0:T(8,128)(2,1)} %bitcast.11, f32[128]{0:T(128)S(1)} %get-tuple-element.7, s32[128]{0:T(128)S(1)} %get-tuple-element.9, f32[128]{0:T(128)S(1)} %get-tuple-element.6, s32[128]{0:T(128)S(1)} %get-tuple-element.8), kind=kOutput, calls=%fused_computation.1 | convolution fusion | flops 503783424 | bytes 1837056 | tf_op jit(solution)/shard_map/dot_general | solution.py:497
  98.0 0.0 copy-done
  98.0 0.7 copy.43
  (3 shorter events, 0.0 us)
Async XLA Ops:
  6.6 88.4 %copy-start.1 = (f32[128,2]{0,1:T(2,128)S(1)}, f32[128,2]{0,1:T(2,128)}, u32[]{:S(2)}) copy-start(f32[128,2]{0,1:T(2,128)} %param.24) | copy-start | bytes 3076
  95.0 2.9 %copy-start = (bf16[128,512]{1,0:T(8,128)(2,1)S(1)}, bf16[128,512]{1,0:T(8,128)(2,1)}, u32[]{:S(2)}) copy-start(bf16[128,512]{1,0:T(8,128)(2,1)} %get-tuple-element.12) | copy-start | bytes 393220
